TPU v7x, 32 devices: a whole 2x2x4 slice. The times are simulated.
32 devices in a mesh: grp: 2 (over y), sp: 4 (over z), tp: 4 (over x, core).
Axes of the slice: x: 2, y: 2, z: 4, core: 2. Of those that a mesh axis runs over, the one named last changes fastest.
Arguments:
- tokens: bfloat16 [2048, 4096], P(('grp', 'sp'), 'tp'), parts along dimension 0, may hold values from -45 to 45
- norm_gain: float32 [2, 4096], replicated, may hold values from 0.1 to 1.9
- value_weight: bfloat16 [2, 4096, 1024], P(None, 'sp', 'tp'), may hold values from -0.09375 to 0.09375
- gate_weight: bfloat16 [2, 4096, 1024], P(None, 'sp', 'tp'), may hold values from -0.09375 to 0.09375
- conv_taps: float32 [2, 31, 1024], P(None, None, 'tp'), may hold values from -4 to 4
- channel_gain: float32 [2, 1024], P(None, 'tp'), may hold values from 0.1 to 1.9
- out_weight: bfloat16 [2, 1024, 4096], P(None, 'sp', 'tp'), may hold values from -0.375 to 0.375
- final_gain: float32 [4096], P('tp'), may hold values from 0.1 to 1.9
Outputs:
- result: bfloat16 [2048, 4096], P(('grp', 'sp'), 'tp'), parts along dimension 0
There are 2 independent parts, one for each index of `grp`. A program takes and returns all parts, laid end to end along the dimension named above; an argument that names none is the same for every part. Nothing has to cross between parts.
All inputs are finite; a program needn't handle non-finite values.
Results may differ from a plain program's by a relative error of at most 0.012.
Values may be sent and summed in bfloat16 or wider, within the bound.
A program may use at most 128 MiB of HBM per device.

v0:
```python
import jax
import jax.numpy as jnp
from jax import lax
from jax.sharding import PartitionSpec as P

D = 4096
C = 1024
LAYERS = 2


def with_halo(block, sides, width):
    for axis, dim in sides:
        count = lax.axis_size(axis)
        forward = [(i, i + 1) for i in range(count - 1)]
        backward = [(target, source) for source, target in forward]
        low = lax.ppermute(
            lax.slice_in_dim(block, block.shape[dim] - width, None, axis=dim), axis, forward
        )
        high = lax.ppermute(lax.slice_in_dim(block, 0, width, axis=dim), axis, backward)
        block = jnp.concatenate([low, block, high], axis=dim)
    return block


def on_device(
    tokens, norm_gain, value_weight, gate_weight, conv_taps, channel_gain, out_weight, final_gain
):
    rows = tokens.shape[0]
    chan_local = channel_gain.shape[1]
    x_state = tokens
    for layer in range(LAYERS):
        xf = x_state.astype(jnp.float32)
        whole = lax.all_gather(x_state, "tp", axis=1, tiled=True).astype(jnp.float32)
        scale = lax.rsqrt(jnp.mean(whole * whole, axis=1, keepdims=True) + 1e-06)
        normed = (whole * scale * norm_gain[layer][None, :]).astype(jnp.bfloat16)
        value = jnp.dot(
            normed,
            lax.all_gather(value_weight[layer], "sp", axis=0, tiled=True),
            preferred_element_type=jnp.float32,
        )
        gate = jnp.dot(
            normed,
            lax.all_gather(gate_weight[layer], "sp", axis=0, tiled=True),
            preferred_element_type=jnp.float32,
        )
        glu = (value * jax.nn.sigmoid(gate)).astype(jnp.bfloat16)
        taps = conv_taps[layer]
        reach = taps.shape[0] // 2
        padded = with_halo(glu, (("sp", 0),), reach).astype(jnp.float32)
        conv = jnp.zeros((rows, chan_local), jnp.float32)
        for tap in range(taps.shape[0]):
            conv = conv + taps[tap][None, :] * padded[tap : tap + rows]
        sums, square_sums = lax.psum((jnp.sum(conv, axis=1), jnp.sum(conv * conv, axis=1)), "tp")
        center = sums / C
        spread = square_sums / C - center * center
        normal_conv = (conv - center[:, None]) * lax.rsqrt(spread + 1e-05)[:, None]
        act_local = jax.nn.silu(normal_conv * channel_gain[layer][None, :]).astype(jnp.bfloat16)
        act = lax.all_gather(act_local, "tp", axis=1, tiled=True)
        branch = jnp.dot(
            act,
            lax.all_gather(out_weight[layer], "sp", axis=0, tiled=True),
            preferred_element_type=jnp.float32,
        )
        x_state = (xf + branch).astype(jnp.bfloat16)
    xf = x_state.astype(jnp.float32)
    squares = lax.psum(jnp.sum(xf * xf, axis=1), "tp")
    scale = lax.rsqrt(squares / D + 1e-06)[:, None]
    return (xf * scale * final_gain[None, :]).astype(jnp.bfloat16)


def solution(mesh):
    placed = (
        P(("grp", "sp"), "tp"),
        P(),
        P(None, "sp", "tp"),
        P(None, "sp", "tp"),
        P(None, None, "tp"),
        P(None, "tp"),
        P(None, "sp", "tp"),
        P("tp"),
    )
    return jax.shard_map(
        on_device, mesh=mesh, in_specs=placed, out_specs=P(("grp", "sp"), "tp"), check_vma=False
    )
```

profile of v0, /device:TPU:0, one launch (start us, length us, event | category | flops | bytes accessed | tf_op | source)
XLA Modules:
  0.0 354.0 jit_solution(3266628995578252068)
XLA Ops:
  7.3 2.3 fusion.139
  9.7 1.1 fusion.138
  11.2 1.1 fusion.137
  12.4 21.8 %all-gather.15.cloned.1.call-done = bf16[256,4096]{1,0:T(8,128)(2,1)} async-done(((bf16[256,1024]{1,0:T(8,128)(2,1)}), bf16[256,4096]{1,0:T(8,128)(2,1)}) %all-gather.15.cloned.1.call-update) | async-done | bytes 2097168 | tf_op jit(solution)/shard_map/all_gather | solution.py:32
  34.2 2.2 fusion
  36.5 45.0 %all-gather.21.cloned.1.call-done = bf16[1,4096,256]{2,1,0:T(8,128)(2,1)} async-done(((bf16[1,1024,256]{2,1,0:T(8,128)(2,1)}), bf16[1,4096,256]{2,1,0:T(8,128)(2,1)}) %all-gather.21.cloned.1.call-update) | async-done | bytes 2097168 | tf_op jit(solution)/shard_map/all_gather | solution.py:42
  81.5 2.4 fusion.42
  83.9 43.7 %all-gather.19.cloned.1.call-done = bf16[1,4096,256]{2,1,0:T(8,128)(2,1)} async-done(((bf16[1,1024,256]{2,1,0:T(8,128)(2,1)}), bf16[1,4096,256]{2,1,0:T(8,128)(2,1)}) %all-gather.19.cloned.1.call-update) | async-done | bytes 2097168 | tf_op jit(solution)/shard_map/all_gather | solution.py:37
  127.5 2.3 fusion.63
  129.9 2.1 collective-permute-start
  132.0 1.3 collective-permute-start.1
  133.3 4.2 %collective-permute-done.1 = bf16[15,256]{1,0:T(8,128)(2,1)S(1)} collective-permute-done((bf16[15,256]{1,0:T(8,128)(2,1)S(1)}, bf16[15,256]{1,0:T(8,128)(2,1)S(1)}, u32[]{:S(2)}, u32[]{:S(2)}) %collective-permute-start.1) | collective-permute-done | bytes 7712 | tf_op jit(solution)/shard_map/ppermute | solution.py:19
  137.6 1.1 fusion.134
  138.7 6.1 %all-reduce.1 = (f32[256]{0:T(256)S(1)}, f32[256]{0:T(256)S(1)}) all-reduce(f32[256]{0:T(256)S(1)} %get-tuple-element.8, f32[256]{0:T(256)S(1)} %get-tuple-element.7), channel_id=1, replica_groups=mesh['grp'=2,'sp'=4,'tp'=4] {'tp'}, use_global_device_ids=true, to_apply=%region_4.0 | all-reduce | flops 512 | bytes 4096 | tf_op jit(solution)/shard_map/psum | solution.py:52
  145.0 7.2 %all_gather.33 = bf16[256,1024]{1,0:T(8,128)(2,1)S(1)} all-gather(bf16[256,256]{1,0:T(8,128)(2,1)S(1)} %multiply_convert_fusion.1), channel_id=1, replica_groups=mesh['grp'=2,'sp'=4,'tp'=4] {'tp'}, dimensions={1}, use_global_device_ids=true | all-gather | bytes 655360 | tf_op jit(solution)/shard_map/all_gather | solution.py:57
  152.2 21.3 %all-gather.23.cloned.1.call-done = bf16[1,1024,1024]{2,1,0:T(8,128)(2,1)} async-done(((bf16[1,256,1024]{2,1,0:T(8,128)(2,1)}), bf16[1,1024,1024]{2,1,0:T(8,128)(2,1)}) %all-gather.23.cloned.1.call-update) | async-done | bytes 2097168 | tf_op jit(solution)/shard_map/all_gather | solution.py:60
  173.5 3.1 fusion.27
  178.7 19.4 %all-gather.17.cloned.1.call-done = bf16[256,4096]{1,0:T(8,128)(2,1)} async-done(((bf16[256,1024]{1,0:T(8,128)(2,1)}), bf16[256,4096]{1,0:T(8,128)(2,1)}) %all-gather.17.cloned.1.call-update) | async-done | bytes 2097168 | tf_op jit(solution)/shard_map/all_gather | solution.py:32
  198.1 2.2 fusion.3
  200.4 44.9 %all-gather.27.cloned.1.call-done = bf16[1,4096,256]{2,1,0:T(8,128)(2,1)} async-done(((bf16[1,1024,256]{2,1,0:T(8,128)(2,1)}), bf16[1,4096,256]{2,1,0:T(8,128)(2,1)}) %all-gather.27.cloned.1.call-update) | async-done | bytes 2097168 | tf_op jit(solution)/shard_map/all_gather | solution.py:42
  245.2 2.4 fusion.57
  247.6 43.7 %all-gather.25.cloned.1.call-done = bf16[1,4096,256]{2,1,0:T(8,128)(2,1)} async-done(((bf16[1,1024,256]{2,1,0:T(8,128)(2,1)}), bf16[1,4096,256]{2,1,0:T(8,128)(2,1)}) %all-gather.25.cloned.1.call-update) | async-done | bytes 2097168 | tf_op jit(solution)/shard_map/all_gather | solution.py:37
  291.3 2.4 fusion.60
  293.7 2.1 collective-permute-start.2
  295.8 1.3 collective-permute-start.3
  297.1 4.2 %collective-permute-done.3 = bf16[15,256]{1,0:T(8,128)(2,1)S(1)} collective-permute-done((bf16[15,256]{1,0:T(8,128)(2,1)S(1)}, bf16[15,256]{1,0:T(8,128)(2,1)S(1)}, u32[]{:S(2)}, u32[]{:S(2)}) %collective-permute-start.3) | collective-permute-done | bytes 7712 | tf_op jit(solution)/shard_map/ppermute | solution.py:19
  301.4 1.2 fusion.133
  302.5 6.1 %all-reduce = (f32[256]{0:T(256)S(1)}, f32[256]{0:T(256)S(1)}) all-reduce(f32[256]{0:T(256)S(1)} %get-tuple-element.6, f32[256]{0:T(256)S(1)} %get-tuple-element.5), channel_id=1, replica_groups=mesh['grp'=2,'sp'=4,'tp'=4] {'tp'}, use_global_device_ids=true, to_apply=%region_9.10 | all-reduce | flops 512 | bytes 4096 | tf_op jit(solution)/shard_map/psum | solution.py:52
  308.8 7.2 %all_gather.38 = bf16[256,1024]{1,0:T(8,128)(2,1)S(1)} all-gather(bf16[256,256]{1,0:T(8,128)(2,1)S(1)} %multiply_convert_fusion), channel_id=1, replica_groups=mesh['grp'=2,'sp'=4,'tp'=4] {'tp'}, dimensions={1}, use_global_device_ids=true | all-gather | bytes 655360 | tf_op jit(solution)/shard_map/all_gather | solution.py:57
  316.0 21.4 %all-gather.29.cloned.1.call-done = bf16[1,1024,1024]{2,1,0:T(8,128)(2,1)} async-done(((bf16[1,256,1024]{2,1,0:T(8,128)(2,1)}), bf16[1,1024,1024]{2,1,0:T(8,128)(2,1)}) %all-gather.29.cloned.1.call-update) | async-done | bytes 2097168 | tf_op jit(solution)/shard_map/all_gather | solution.py:60
  337.4 2.4 fusion.66
  339.8 6.4 %psum.39 = f32[256]{0:T(256)S(1)} all-reduce(f32[256]{0:T(256)S(1)} %get-tuple-element.95), channel_id=1, replica_groups=mesh['grp'=2,'sp'=4,'tp'=4] {'tp'}, use_global_device_ids=true, to_apply=%region_11.12 | all-reduce | flops 256 | bytes 2048 | tf_op jit(solution)/shard_map/psum | solution.py:65
  (56 shorter events, 5.0 us)
Async XLA Ops:
  6.5 3.1 copy-start.2
  6.5 27.7 %all-gather.15.cloned.1.call-start = ((), (), s32[]{:S(2)}) async-start(), calls=%async_computation | async-start | bytes 2621440 | tf_op jit(solution)/shard_map/all_gather | solution.py:32
  7.3 74.2 %all-gather.21.cloned.1.call-start = ((), (), s32[]{:S(2)}) async-start(), calls=%async_computation.3 | async-start | bytes 2621440 | tf_op jit(solution)/shard_map/all_gather | solution.py:42
  9.6 1.6 copy-start.3
  9.6 117.9 %all-gather.19.cloned.1.call-start = ((), (), s32[]{:S(2)}) async-start(), calls=%async_computation.2 | async-start | bytes 2621440 | tf_op jit(solution)/shard_map/all_gather | solution.py:37
  10.8 1.5 copy-start.6
  10.8 1.6 copy-start.7
  10.8 162.7 %all-gather.23.cloned.1.call-start = ((), (), s32[]{:S(2)}) async-start(), calls=%async_computation.4 | async-start | bytes 2621440 | tf_op jit(solution)/shard_map/all_gather | solution.py:60
  12.3 185.9 %all-gather.17.cloned.1.call-start = ((), (), s32[]{:S(2)}) async-start(), calls=%async_computation.1 | async-start | bytes 2621440 | tf_op jit(solution)/shard_map/all_gather | solution.py:32
  34.2 47.3 %copy-start = (bf16[256,4096]{1,0:T(8,128)(2,1)S(1)}, bf16[256,4096]{1,0:T(8,128)(2,1)}, u32[]{:S(2)}) copy-start(bf16[256,4096]{1,0:T(8,128)(2,1)} %all-gather.15.cloned.1.call-done) | copy-start | bytes 6291460
  83.9 49.4 %copy-start.9 = (f32[2,256]{1,0:T(2,128)S(1)}, f32[2,256]{1,0:T(2,128)}, u32[]{:S(2)}) copy-start(f32[2,256]{1,0:T(2,128)} %param.13) | copy-start | bytes 6148
  129.9 3.4 collective-permute-start
  132.0 5.5 %collective-permute-start.1 = (bf16[15,256]{1,0:T(8,128)(2,1)S(1)}, bf16[15,256]{1,0:T(8,128)(2,1)S(1)}, u32[]{:S(2)}, u32[]{:S(2)}) collective-permute-start(bf16[15,256]{1,0:T(8,128)(2,1)S(1)} %get-tuple-element.24), channel_id=1, source_target_pairs={{4,0},{8,4},{12,8},{5,1},{9,5},{13,9},{6,2},{10,6},{14,10},{7,3},{... | collective-permute-start | bytes 23048 | tf_op jit(solution)/shard_map/ppermute | solution.py:19
  137.6 35.9 %copy-start.4 = (bf16[256,1024]{1,0:T(8,128)(2,1)S(1)}, bf16[256,1024]{1,0:T(8,128)(2,1)}, u32[]{:S(2)}) copy-start(bf16[256,1024]{1,0:T(8,128)(2,1)} %param.8) | copy-start | bytes 1572868
  176.6 68.6 %all-gather.27.cloned.1.call-start = ((), (), s32[]{:S(2)}) async-start(), calls=%async_computation.6 | async-start | bytes 2621440 | tf_op jit(solution)/shard_map/all_gather | solution.py:42
  177.2 114.1 %all-gather.25.cloned.1.call-start = ((), (), s32[]{:S(2)}) async-start(), calls=%async_computation.5 | async-start | bytes 2621440 | tf_op jit(solution)/shard_map/all_gather | solution.py:37
  177.9 159.4 %all-gather.29.cloned.1.call-start = ((), (), s32[]{:S(2)}) async-start(), calls=%async_computation.7 | async-start | bytes 2621440 | tf_op jit(solution)/shard_map/all_gather | solution.py:60
  198.1 47.1 %copy-start.1 = (bf16[256,4096]{1,0:T(8,128)(2,1)S(1)}, bf16[256,4096]{1,0:T(8,128)(2,1)}, u32[]{:S(2)}) copy-start(bf16[256,4096]{1,0:T(8,128)(2,1)} %all-gather.17.cloned.1.call-done) | copy-start | bytes 6291460
  293.7 3.4 collective-permute-start.2
  295.8 5.5 %collective-permute-start.3 = (bf16[15,256]{1,0:T(8,128)(2,1)S(1)}, bf16[15,256]{1,0:T(8,128)(2,1)S(1)}, u32[]{:S(2)}, u32[]{:S(2)}) collective-permute-start(bf16[15,256]{1,0:T(8,128)(2,1)S(1)} %get-tuple-element.22), channel_id=1, source_target_pairs={{4,0},{8,4},{12,8},{5,1},{9,5},{13,9},{6,2},{10,6},{14,10},{7,3},{... | collective-permute-start | bytes 23048 | tf_op jit(solution)/shard_map/ppermute | solution.py:19
  301.4 36.0 %copy-start.5 = (bf16[256,1024]{1,0:T(8,128)(2,1)S(1)}, bf16[256,1024]{1,0:T(8,128)(2,1)}, u32[]{:S(2)}) copy-start(bf16[256,1024]{1,0:T(8,128)(2,1)} %fusion.27) | copy-start | bytes 1572868
  316.0 30.3 %copy-start.8 = (f32[1024]{0:T(1024)S(1)}, f32[1024]{0:T(1024)}, u32[]{:S(2)}) copy-start(f32[1024]{0:T(1024)} %param.15) | copy-start | bytes 12292
Sparse Core Ops, SparseCore 0:
  8.9 25.2 all-gather.14
  35.8 45.6 all-gather.20
  83.0 44.4 all-gather.18
  129.0 44.4 all-gather.22
  176.7 21.3 all-gather.16
  199.6 45.6 all-gather.26
  246.8 44.4 all-gather.24
  292.9 44.4 all-gather.28
where the time goes:
time: 355 us; the launch traced here: 354 us
  waiting for transfers between devices  272 us (77%)
  blocking collectives  32.8 us (9%)
  matrix products  15 us (4%)
  between operations  13.7 us (4%)
  other arithmetic  8.24 us (2%)
  starting transfers between devices  7.02 us (2%)
  local copies, waits for them, and re-layouts  4.93 us (1%)
    all_gather x2, waiting for transfers between devices, on_device(): lax.all_gather(gate_weight[layer], 'sp', axis=0, tiled=True)  89.9 us
    all_gather x2, waiting for transfers between devices, on_device(): lax.all_gather(value_weight[layer], 'sp', axis=0, tiled=True)  87.3 us
    all_gather x2, waiting for transfers between devices, on_device(): lax.all_gather(out_weight[layer], 'sp', axis=0, tiled=True)  42.7 us
    all_gather x2, waiting for transfers between devices, on_device(): lax.all_gather(x_state, 'tp', axis=1, tiled=True).astype(jnp.float32)  41.2 us
    all_gather x2, blocking collectives, on_device(): act = lax.all_gather(act_local, 'tp', axis=1, tiled=True)  14.3 us
    psum x2, blocking collectives, on_device(): lax.psum((jnp.sum(conv, axis=1), jnp.sum(conv * conv, axis=1)), 'tp')  12.1 us
    ppermute x2, waiting for transfers between devices, with_halo(): lax.ppermute(lax.slice_in_dim(block, 0, width, axis=dim), axis, backward)  8.39 us
  transfers between devices with their start and end apart: 12, of which 10 were waited for; matrix products, arithmetic and copies ran while one was open for 6% of the time, Pallas kernels for 0%

commit v1 on v0

v1 whole, which is shorter than its diff:
```python
import functools

import jax
import jax.numpy as jnp
from jax import lax
from jax.experimental import pallas as pl
from jax.experimental.pallas import tpu as pltpu
from jax.sharding import PartitionSpec as P

MESH = pl.DeviceIdType.MESH
Q = 2
PAD = 16


def kernel(
    G, n, T, L,
    tokens, gain, value_w, gate_w, taps, cgain, out_w, fgain,
    result,
    wvg, wo, xg, xn, acc, pad, padf, conv, stat, actg, x_state,
    local_sem, z_recv, right_send, left_send, y_send, y_recv,
    x_send, x_recv, a_send, a_recv, s_send, s_recv, h_send, h_recv,
):
    g, s, t = lax.axis_index("grp"), lax.axis_index("sp"), lax.axis_index("tp")
    rows, width = tokens.shape
    depth, chans = value_w.shape[1:]
    out_rows = out_w.shape[1]
    half = chans // G
    out_half = width // G
    reach = taps.shape[1] // 2
    n_taps = taps.shape[1]
    D = width * T
    C = chans * T
    chunk = depth // Q
    pieces = Q + 1
    f32, bf16 = jnp.float32, jnp.bfloat16

    def piece(p, h, j):
        layer, q = p // pieces, p % pieces
        if q < Q:
            start = pl.multiple_of(j * depth + q * chunk, chunk)
            return wvg.at[layer, h, pl.ds(start, chunk), :]
        return wo.at[layer, h, pl.ds(pl.multiple_of(j * out_rows, out_rows), out_rows), :]

    locals_ = [pltpu.make_async_copy(tokens, xg.at[0, t], local_sem.at[0])]
    own_rows = pl.ds(pl.multiple_of(s * depth, depth), depth)
    own_out = pl.ds(pl.multiple_of(s * out_rows, out_rows), out_rows)
    count = 1
    per_layer = []
    for layer in range(L):
        group = []
        for h in range(G):
            for k, w in enumerate((value_w, gate_w)):
                group.append(pltpu.make_async_copy(
                    w.at[layer, :, pl.ds(h * half, half)],
                    wvg.at[layer, h, own_rows, pl.ds(k * half, half)],
                    local_sem.at[count]))
                count += 1
            group.append(pltpu.make_async_copy(
                out_w.at[layer, :, pl.ds(h * out_half, out_half)],
                wo.at[layer, h, own_out, :], local_sem.at[count]))
            count += 1
        per_layer.append(group)
    for c in locals_ + sum(per_layer, []):
        c.start()

    barrier = pltpu.get_barrier_semaphore()
    for d in range(1, T):
        pl.semaphore_signal(barrier, inc=1, device_id={"tp": lax.rem(t + d, T)}, device_id_type=MESH)
    for d in range(1, G):
        pl.semaphore_signal(barrier, inc=1, device_id={"grp": lax.rem(g + d, G)}, device_id_type=MESH)

    @pl.when(s > 0)
    def _():
        pl.semaphore_signal(barrier, inc=1, device_id={"sp": s - 1}, device_id_type=MESH)

    @pl.when(s < n - 1)
    def _():
        pl.semaphore_signal(barrier, inc=1, device_id={"sp": s + 1}, device_id_type=MESH)

    sides = jnp.where(s > 0, 1, 0) + jnp.where(s < n - 1, 1, 0)
    pl.semaphore_wait(barrier, (T - 1) + (G - 1) + sides)

    def right(p, j):
        r = piece(p, g, j)
        return pltpu.make_async_remote_copy(
            src_ref=r, dst_ref=r, send_sem=right_send.at[p, j], recv_sem=z_recv.at[p, j],
            device_id={"sp": s + 1}, device_id_type=MESH)

    def left(p, j):
        r = piece(p, g, j)
        return pltpu.make_async_remote_copy(
            src_ref=r, dst_ref=r, send_sem=left_send.at[p, j], recv_sem=z_recv.at[p, j],
            device_id={"sp": s - 1}, device_id_type=MESH)

    def across(p, j, d, h):
        r = piece(p, h, j)
        return pltpu.make_async_remote_copy(
            src_ref=r, dst_ref=r, send_sem=y_send.at[p, j, d - 1], recv_sem=y_recv.at[p, j, d - 1],
            device_id={"grp": lax.rem(g + d, G)}, device_id_type=MESH)

    batches = []
    for layer in range(L):
        base = layer * pieces
        batches += [list(range(base, base + Q)), [base + Q]]

    def own_right(ps):
        for p in ps:
            right(p, s).start()

    def own_left(ps):
        for p in ps:
            left(p, s).start()

    def relay(b, low, high):
        low, high = min(low, n - 1), min(high, n - 1)
        following = batches[b + 1] if b + 1 < len(batches) else []

        def step(k, carry):
            for p in batches[b]:
                from_left, from_right = s - 1 - k, s + 1 + k

                @pl.when(from_left >= 0)
                def _():
                    j = jnp.maximum(from_left, 0)
                    right(p, j).wait_recv()

                    @pl.when(s < n - 1)
                    def _():
                        right(p, j).start()

                    for d in range(1, G):
                        across(p, j, d, g).start()

                @pl.when(from_right < n)
                def _():
                    j = jnp.minimum(from_right, n - 1)
                    left(p, j).wait_recv()

                    @pl.when(s > 0)
                    def _():
                        left(p, j).start()

                    for d in range(1, G):
                        across(p, j, d, g).start()

            @pl.when((k == s - 1) & (s < n - 1))
            def _():
                own_right(following)

            @pl.when((k == n - 2 - s) & (s > 0))
            def _():
                own_left(following)

            return carry

        if high > low:
            lax.fori_loop(low, high, step, 0)

    def others(fn):
        def step(j, carry):
            @pl.when(j != s)
            def _():
                fn(j)
            return carry
        lax.fori_loop(0, n, step, 0)

    def wait_across(b):
        for p in batches[b]:
            for d in range(1, G):
                others(lambda j: across(p, j, d, lax.rem(g + G - d, G)).wait_recv())

    def spread(buf, layer, send, recv):
        def copy(bit, m):
            block = buf.at[layer, t ^ m]
            return pltpu.make_async_remote_copy(
                src_ref=block, dst_ref=block, send_sem=send.at[layer, bit + m], recv_sem=recv.at[layer, bit + m],
                device_id={"tp": t ^ bit}, device_id_type=MESH)

        def arrival(bit, m):
            block = buf.at[layer, t ^ bit ^ m]
            return pltpu.make_async_remote_copy(
                src_ref=block, dst_ref=block, send_sem=send.at[layer, bit + m], recv_sem=recv.at[layer, bit + m],
                device_id={"tp": t ^ bit}, device_id_type=MESH)

        bits = []
        bit = T // 2
        while bit >= 1:
            bits.append(bit)
            bit //= 2

        def begin():
            for bit in bits:
                copy(bit, 0).start()

        def finish():
            have, sent = [0], []
            for i, bit in enumerate(bits):
                for m in have:
                    arrival(bit, m).wait_recv()
                    sent.append((bit, m))
                    for lower in bits[i + 1:]:
                        copy(lower, m ^ bit).start()
                have = have + [m ^ bit for m in have]
            return lambda: [copy(bit, m).wait_send() for bit, m in sent]

        return begin, finish

    def exchange(index, columns):
        lane = lax.broadcasted_iota(jnp.int32, (rows, 128), 1)
        tile = jnp.zeros((rows, 128), f32)
        for i, column in enumerate(columns):
            tile = jnp.where(lane == i, column, tile)
        stat[index, 0] = tile.T[:8, :]

        def copy(d):
            return pltpu.make_async_remote_copy(
                src_ref=stat.at[index, 0], dst_ref=stat.at[index, d],
                send_sem=s_send.at[index, d - 1], recv_sem=s_recv.at[index, d - 1],
                device_id={"tp": lax.rem(t + d, T)}, device_id_type=MESH)

        for d in range(1, T):
            copy(d).start()

        def total():
            for d in range(1, T):
                copy(d).wait_recv()
            sums = stat[index, 0]
            for d in range(1, T):
                sums = sums + stat[index, d]
            wide = jnp.concatenate([sums, jnp.zeros((120, rows), f32)], axis=0).T
            for d in range(1, T):
                copy(d).wait_send()
            return [wide[:, i:i + 1] for i in range(len(columns))]

        return total

    def normalize(layer):
        def squares(j, total):
            part = xg[layer, j].astype(f32)
            return total + jnp.sum(part * part, axis=1, keepdims=True)
        mean = lax.fori_loop(0, T, squares, jnp.zeros((rows, 1), f32)) / D
        scale = lax.rsqrt(mean + 1e-06)

        def body(j, carry):
            xn[j] = (xg[layer, j].astype(f32) * scale * gain[layer * T + j][None, :]).astype(bf16)
            return carry
        lax.fori_loop(0, T, body, 0)

    def project(layer):
        for h in range(G):
            def body(j, carry):
                block = wvg[layer, h, pl.ds(pl.multiple_of(j * width, width), width), :]
                part = jnp.dot(xn[j], block, preferred_element_type=f32)

                @pl.when(j == 0)
                def _():
                    acc[...] = part

                @pl.when(j > 0)
                def _():
                    acc[...] += part
                return carry
            lax.fori_loop(0, T, body, 0)
            glu = acc[:, :half] * jax.nn.sigmoid(acc[:, half:])
            pad[layer, PAD:PAD + rows, h * half:(h + 1) * half] = glu.astype(bf16)

    for c in locals_:
        c.wait()
    spreads = [spread(xg, layer, x_send, x_recv) for layer in range(L)]
    spreads[0][0]()
    for c in sum(per_layer, []):
        c.wait()

    @pl.when(s < n - 1)
    def _():
        own_right(batches[0])

    @pl.when(s > 0)
    def _():
        own_left(batches[0])

    @pl.when((s == 0) & (s < n - 1))
    def _():
        for b in batches[1:]:
            own_right(b)

    @pl.when((s == n - 1) & (s > 0))
    def _():
        for b in batches[1:]:
            own_left(b)

    x_state[...] = tokens_f32(tokens, xg, t)
    drains = []

    for layer in range(L):
        first, second = 2 * layer, 2 * layer + 1
        relay(first, 0, 1)
        drains.append(spreads[layer][1]())
        normalize(layer)
        relay(first, 1, n)
        wait_across(first)
        project(layer)

        def to_right():
            return pltpu.make_async_remote_copy(
                src_ref=pad.at[layer, pl.ds(rows, PAD), :], dst_ref=pad.at[layer, pl.ds(0, PAD), :],
                send_sem=h_send.at[layer, 0], recv_sem=h_recv.at[layer, 0],
                device_id={"sp": s + 1}, device_id_type=MESH)

        def to_left():
            return pltpu.make_async_remote_copy(
                src_ref=pad.at[layer, pl.ds(PAD, PAD), :], dst_ref=pad.at[layer, pl.ds(PAD + rows, PAD), :],
                send_sem=h_send.at[layer, 1], recv_sem=h_recv.at[layer, 1],
                device_id={"sp": s - 1}, device_id_type=MESH)

        @pl.when(s < n - 1)
        def _():
            to_right().start()

        @pl.when(s > 0)
        def _():
            to_left().start()

        @pl.when(s == 0)
        def _():
            pad[layer, 0:PAD, :] = jnp.zeros((PAD, chans), bf16)

        @pl.when(s == n - 1)
        def _():
            pad[layer, PAD + rows:, :] = jnp.zeros((PAD, chans), bf16)

        relay(second, 0, 1)

        @pl.when(s > 0)
        def _():
            to_right().wait_recv()

        @pl.when(s < n - 1)
        def _():
            to_left().wait_recv()

        padf[...] = pad[layer].astype(f32)
        block = 64
        sums, squares = [], []
        for r in range(0, rows, block):
            total = jnp.zeros((block, chans), f32)
            for k in range(n_taps):
                start = r + PAD - reach + k
                total = total + taps[layer, k][None, :] * padf[start:start + block, :]
            conv[r:r + block, :] = total
            sums.append(jnp.sum(total, axis=1, keepdims=True))
            squares.append(jnp.sum(total * total, axis=1, keepdims=True))
        totals = exchange(layer, [jnp.concatenate(sums, 0), jnp.concatenate(squares, 0)])
        relay(second, 1, 2)
        total, square = totals()
        center = total / C
        spread_ = square / C - center * center
        normal = (conv[...] - center) * lax.rsqrt(spread_ + 1e-05)
        actg[layer, t] = jax.nn.silu(normal * cgain[layer][None, :]).astype(bf16)
        act_begin, act_finish = spread(actg, layer, a_send, a_recv)
        act_begin()
        drains.append(act_finish())
        relay(second, 2, n)
        wait_across(second)
        for h in range(G):
            part = None
            for j in range(T):
                term = jnp.dot(actg[layer, j], wo[layer, h, j * chans:(j + 1) * chans, :], preferred_element_type=f32)
                part = term if part is None else part + term
            cols = slice(h * out_half, (h + 1) * out_half)
            x_state[:, cols] = (x_state[:, cols] + part).astype(bf16).astype(f32)
        if layer + 1 < L:
            xg[layer + 1, t] = x_state[...].astype(bf16)
            spreads[layer + 1][0]()

        @pl.when(s < n - 1)
        def _():
            to_right().wait_send()

        @pl.when(s > 0)
        def _():
            to_left().wait_send()

    xf = x_state[...]
    totals = exchange(L, [jnp.sum(xf * xf, axis=1, keepdims=True)])

    for drain in drains:
        drain()

    def drain_step(j, carry):
        for p in range(L * pieces):
            @pl.when((j <= s) & (s < n - 1))
            def _():
                right(p, j).wait_send()

            @pl.when((j >= s) & (s > 0))
            def _():
                left(p, j).wait_send()

            @pl.when(j != s)
            def _():
                for d in range(1, G):
                    across(p, j, d, g).wait_send()
        return carry
    lax.fori_loop(0, n, drain_step, 0)

    (total,) = totals()
    scale = lax.rsqrt(total / D + 1e-06)
    result[...] = (x_state[...] * scale * fgain[...]).astype(bf16)


def tokens_f32(tokens, xg, t):
    return xg[0, t].astype(jnp.float32)


def on_device(G, n, T, tokens, norm_gain, value_w, gate_w, taps, cgain, out_w, fgain):
    L = norm_gain.shape[0]
    rows, width = tokens.shape
    depth, chans = value_w.shape[1:]
    D, C = width * T, chans * T
    bf16, f32 = jnp.bfloat16, jnp.float32
    dma = pltpu.SemaphoreType.DMA
    vmem = pl.BlockSpec(memory_space=pltpu.VMEM)
    hbm = pl.BlockSpec(memory_space=pl.ANY)
    P_ = L * (Q + 1)
    peers = max(G - 1, 1)
    return pl.pallas_call(
        functools.partial(kernel, G, n, T, L),
        out_shape=jax.ShapeDtypeStruct((rows, width), bf16),
        in_specs=[hbm, vmem, hbm, hbm, vmem, vmem, hbm, vmem],
        out_specs=vmem,
        scratch_shapes=[
            pltpu.VMEM((L, G, D, 2 * chans // G), bf16),
            pltpu.VMEM((L, G, C, width // G), bf16),
            pltpu.VMEM((L, T, rows, width), bf16),
            pltpu.VMEM((T, rows, width), bf16),
            pltpu.VMEM((rows, 2 * chans // G), f32),
            pltpu.VMEM((L, rows + 2 * PAD, chans), bf16),
            pltpu.VMEM((rows + 2 * PAD, chans), f32),
            pltpu.VMEM((rows, chans), f32),
            pltpu.VMEM((L + 1, T, 8, rows), f32),
            pltpu.VMEM((L, T, rows, chans), bf16),
            pltpu.VMEM((rows, width), f32),
            dma((1 + L * G * 3,)),
            dma((P_, n)), dma((P_, n)), dma((P_, n)),
            dma((P_, n, peers)), dma((P_, n, peers)),
            dma((L, T)), dma((L, T)), dma((L, T)), dma((L, T)),
            dma((L + 1, T)), dma((L + 1, T)),
            dma((L, 2)), dma((L, 2)),
        ],
        compiler_params=pltpu.CompilerParams(
            collective_id=0, has_side_effects=True, vmem_limit_bytes=56 * 2**20
        ),
    )(tokens, norm_gain.reshape(L * T, width), value_w, gate_w, taps, cgain, out_w, fgain.reshape(1, width))


def solution(mesh):
    placed = (
        P(("grp", "sp"), "tp"),
        P(),
        P(None, "sp", "tp"),
        P(None, "sp", "tp"),
        P(None, None, "tp"),
        P(None, "tp"),
        P(None, "sp", "tp"),
        P("tp"),
    )
    G, n, T = (mesh.shape[a] for a in ("grp", "sp", "tp"))
    return jax.shard_map(
        functools.partial(on_device, G, n, T),
        mesh=mesh, in_specs=placed, out_specs=P(("grp", "sp"), "tp"), check_vma=False,
    )
```

time: 355 us -> 140 us (0.39)
  waiting for transfers between devices: 272 us -> 0 us
  Pallas kernels: 0 us -> 136 us
  blocking collectives: 32.8 us -> 0 us
  matrix products: 15 us -> 0 us
  between operations: 13.7 us -> 0.01 us
  other arithmetic: 8.24 us -> 0 us
  starting transfers between devices: 7.02 us -> 0 us
    all_gather x8 -> x0, waiting for transfers between devices: 261 us -> none  [the longest x2 89.9 us: on_device(): lax.all_gather(gate_weight[layer], 'sp', axis=0, tiled=True)]
    pallas_call x0 -> x1, Pallas kernels: none -> 136 us  [on_device(): pl.pallas_call(functools.partial(kernel, G, n, T, L), out_shape=jax.Shape...]
    psum x3 -> x0, blocking collectives: 18.5 us -> none  [the longest x2 12.1 us: on_device(): lax.psum((jnp.sum(conv, axis=1), jnp.sum(conv * conv, axis=1)), 'tp')]
    dot_general x6 -> x0, matrix products: 15 us -> none  [the longest x2 5.56 us: on_device(): jnp.dot(act, lax.all_gather(out_weight[layer], 'sp', axis=0, tiled=True),...]
    all_gather x2 -> x0, blocking collectives: 14.3 us -> none  [on_device(): act = lax.all_gather(act_local, 'tp', axis=1, tiled=True)]
    ppermute x4 -> x0, waiting for transfers between devices: 8.43 us -> none  [the longest x2 8.39 us: with_halo(): lax.ppermute(lax.slice_in_dim(block, 0, width, axis=dim), axis, backward)]
    reduce_sum x4 -> x0, other arithmetic: 6.78 us -> none  [the longest x2 4.47 us: on_device(): scale = lax.rsqrt(jnp.mean(whole * whole, axis=1, keepdims=True) + 1e-06)]
    ppermute x4 -> x0, starting transfers between devices: 6.73 us -> none  [the longest x2 4.15 us: with_halo(): lax.ppermute(lax.slice_in_dim(block, block.shape[dim] - width, None, axis...]
  transfers between devices with their start and end apart: 12 -> 0, of which waited for: 10 -> 0; matrix products, arithmetic and copies ran while one was open for 6% -> 0% of each run, Pallas kernels for 0% -> 0%
where the time goes in v1:
time: 140 us; the launch traced here: 139 us
  Pallas kernels  136 us (97%)
  local copies, waits for them, and re-layouts  3.91 us (3%)
    pallas_call x1, Pallas kernels, on_device(): pl.pallas_call(functools.partial(kernel, G, n, T, L), out_shape=jax.Shape...  136 us

profile of v1, /device:TPU:0, one launch (start us, length us, event | category | flops | bytes accessed | tf_op | source)
XLA Modules:
  0.0 139.5 jit_solution(10693586890768770153)
XLA Ops:
  0.0 0.0 copy-start
  0.0 1.4 %reshape.6.gain = f32[8,1024]{1,0:T(8,128)} reshape(f32[2,4096]{1,0:T(2,128)} %param.9) | data formatting | bytes 65536 | tf_op jit(solution)/shard_map/reshape | solution.py:454
  1.4 0.0 copy-done
  1.4 0.6 copy.9.taps
  2.0 135.5 %shard_map.82 = bf16[256,1024]{1,0:T(8,128)(2,1)} custom-call(bf16[256,1024]{1,0:T(8,128)(2,1)} %tokens.1, f32[8,1024]{1,0:T(8,128)} %reshape.6.gain, bf16[2,1024,256]{2,1,0:T(8,128)(2,1)} %value_w.1, bf16[2,1024,256]{2,1,0:T(8,128)(2,1)} %gate_w.1, f32[2,31,256]{2,1,0:T(8,128)} %copy.9.taps, f32[2,256]{1,0:T(2,128)} %cgain.1, bf16[2,256,1024]{2,1,0:T(8,128)(2,1)} %out_w.1, ...), custom_call_target="tpu_custom_call" | custom-call | tf_op jit(solution)/shard_map/pallas_call | solution.py:427
  137.6 1.9 %copy.11 = bf16[256,1024]{1,0:T(8,128)(2,1)} copy(bf16[256,1024]{1,0:T(8,128)(2,1)} %shard_map.82) | data formatting | bytes 1048576
Async XLA Ops:
  0.0 1.4 %copy-start = (f32[2,31,256]{2,0,1:T(2,128)S(1)}, f32[2,31,256]{2,0,1:T(2,128)}, u32[]{:S(2)}) copy-start(f32[2,31,256]{2,0,1:T(2,128)} %param.12) | copy-start | bytes 190468

commit v2 on v1

--- a/solution.py
+++ b/solution.py
@@ -16,9 +16,9 @@
     G, n, T, L,
     tokens, gain, value_w, gate_w, taps, cgain, out_w, fgain,
     result,
-    wvg, wo, xg, xn, acc, pad, padf, conv, stat, actg, x_state,
+    wvg, wo, xg, xn, glu_out, acc, pad, padf, conv, stat, actg, x_state,
     local_sem, z_recv, right_send, left_send, y_send, y_recv,
-    x_send, x_recv, a_send, a_recv, s_send, s_recv, h_send, h_recv,
+    x_send, x_recv, a_send, a_recv, s_send, s_recv, h_send, h_recv, f_send, f_recv,
 ):
     g, s, t = lax.axis_index("grp"), lax.axis_index("sp"), lax.axis_index("tp")
     rows, width = tokens.shape
@@ -33,6 +33,30 @@
     chunk = depth // Q
     pieces = Q + 1
     f32, bf16 = jnp.float32, jnp.bfloat16
+    helped = n >= 4
+    last = n - 1
+    is_end = (s == 0) | (s == last)
+    helper = (s == 1) | (s == last - 1)
+    end = jnp.where(s == 1, 0, last)
+    inward = jnp.where(s == 0, 1, last - 1)
+
+    def ends_out(p):
+        return helped and p < Q
+
+    def to_right_ok(p):
+        return s < last - 1 if ends_out(p) else s < last
+
+    def to_left_ok(p):
+        return s > 1 if ends_out(p) else s > 0
+
+    def takes(p):
+        return jnp.logical_not(is_end) if ends_out(p) else s >= 0
+
+    def by_grp(p, j):
+        ok = takes(p) & (j != s)
+        if helped and p == 0:
+            ok = ok & jnp.logical_not((s == 1) & (j == 0)) & jnp.logical_not((s == last - 1) & (j == last))
+        return ok
 
     def piece(p, h, j):
         layer, q = p // pieces, p % pieces
@@ -111,6 +135,23 @@
         for p in ps:
             left(p, s).start()
 
+    def end_rows(target):
+        return pltpu.make_async_remote_copy(
+            src_ref=xg.at[0, t], dst_ref=xg.at[L, t], send_sem=f_send.at[0], recv_sem=f_recv.at[0],
+            device_id={"sp": target}, device_id_type=MESH)
+
+    def end_piece(d, h, j, target):
+        r = piece(0, h, j)
+        return pltpu.make_async_remote_copy(
+            src_ref=r, dst_ref=r, send_sem=f_send.at[d], recv_sem=f_recv.at[d],
+            device_id={"sp": target}, device_id_type=MESH)
+
+    def end_glu(target):
+        return pltpu.make_async_remote_copy(
+            src_ref=glu_out, dst_ref=pad.at[0, pl.ds(PAD, rows), :],
+            send_sem=f_send.at[G], recv_sem=f_recv.at[G],
+            device_id={"sp": target}, device_id_type=MESH)
+
     def relay(b, low, high):
         low, high = min(low, n - 1), min(high, n - 1)
         following = batches[b + 1] if b + 1 < len(batches) else []
@@ -119,35 +160,39 @@
             for p in batches[b]:
                 from_left, from_right = s - 1 - k, s + 1 + k
 
-                @pl.when(from_left >= 0)
+                @pl.when((from_left >= 0) & takes(p))
                 def _():
                     j = jnp.maximum(from_left, 0)
                     right(p, j).wait_recv()
 
-                    @pl.when(s < n - 1)
+                    @pl.when(to_right_ok(p))
                     def _():
                         right(p, j).start()
 
-                    for d in range(1, G):
-                        across(p, j, d, g).start()
-
-                @pl.when(from_right < n)
+                    @pl.when(by_grp(p, j))
+                    def _():
+                        for d in range(1, G):
+                            across(p, j, d, g).start()
+
+                @pl.when((from_right < n) & takes(p))
                 def _():
                     j = jnp.minimum(from_right, n - 1)
                     left(p, j).wait_recv()
 
-                    @pl.when(s > 0)
+                    @pl.when(to_left_ok(p))
                     def _():
                         left(p, j).start()
 
-                    for d in range(1, G):
-                        across(p, j, d, g).start()
-
-            @pl.when((k == s - 1) & (s < n - 1))
+                    @pl.when(by_grp(p, j))
+                    def _():
+                        for d in range(1, G):
+                            across(p, j, d, g).start()
+
+            @pl.when((k == s - 1) & (s < (last - 1 if helped and b < 2 else last)))
             def _():
                 own_right(following)
 
-            @pl.when((k == n - 2 - s) & (s > 0))
+            @pl.when((k == n - 2 - s) & (s > (1 if helped and b < 2 else 0)))
             def _():
                 own_left(following)
 
@@ -156,18 +201,15 @@
         if high > low:
             lax.fori_loop(low, high, step, 0)
 
-    def others(fn):
-        def step(j, carry):
-            @pl.when(j != s)
-            def _():
-                fn(j)
-            return carry
-        lax.fori_loop(0, n, step, 0)
-
     def wait_across(b):
         for p in batches[b]:
-            for d in range(1, G):
-                others(lambda j: across(p, j, d, lax.rem(g + G - d, G)).wait_recv())
+            def step(j, carry):
+                @pl.when(by_grp(p, j))
+                def _():
+                    for d in range(1, G):
+                        across(p, j, d, lax.rem(g + G - d, G)).wait_recv()
+                return carry
+            lax.fori_loop(0, n, step, 0)
 
     def spread(buf, layer, send, recv):
         def copy(bit, m):
@@ -234,23 +276,23 @@
 
         return total
 
-    def normalize(layer):
+    def normalize(layer, held, into):
         def squares(j, total):
-            part = xg[layer, j].astype(f32)
+            part = xg[held, j].astype(f32)
             return total + jnp.sum(part * part, axis=1, keepdims=True)
         mean = lax.fori_loop(0, T, squares, jnp.zeros((rows, 1), f32)) / D
         scale = lax.rsqrt(mean + 1e-06)
 
         def body(j, carry):
-            xn[j] = (xg[layer, j].astype(f32) * scale * gain[layer * T + j][None, :]).astype(bf16)
+            xn[into, j] = (xg[held, j].astype(f32) * scale * gain[layer * T + j][None, :]).astype(bf16)
             return carry
         lax.fori_loop(0, T, body, 0)
 
-    def project(layer):
+    def project(layer, held, put):
         for h in range(G):
             def body(j, carry):
                 block = wvg[layer, h, pl.ds(pl.multiple_of(j * width, width), width), :]
-                part = jnp.dot(xn[j], block, preferred_element_type=f32)
+                part = jnp.dot(xn[held, j], block, preferred_element_type=f32)
 
                 @pl.when(j == 0)
                 def _():
@@ -262,7 +304,7 @@
                 return carry
             lax.fori_loop(0, T, body, 0)
             glu = acc[:, :half] * jax.nn.sigmoid(acc[:, half:])
-            pad[layer, PAD:PAD + rows, h * half:(h + 1) * half] = glu.astype(bf16)
+            put(h, glu.astype(bf16))
 
     for c in locals_:
         c.wait()
@@ -271,13 +313,32 @@
     for c in sum(per_layer, []):
         c.wait()
 
-    @pl.when(s < n - 1)
+    @pl.when(to_right_ok(0))
     def _():
         own_right(batches[0])
 
-    @pl.when(s > 0)
+    @pl.when(to_left_ok(0))
     def _():
         own_left(batches[0])
+
+    if helped:
+        @pl.when(is_end)
+        def _():
+            end_rows(inward).start()
+            for d in range(1, G):
+                end_piece(d, lax.rem(g + d, G), s, inward).start()
+
+        @pl.when(s == last - 1)
+        def _():
+            own_right(batches[1])
+            if L > 1:
+                own_right(batches[2])
+
+        @pl.when(s == 1)
+        def _():
+            own_left(batches[1])
+            if L > 1:
+                own_left(batches[2])
 
     @pl.when((s == 0) & (s < n - 1))
     def _():
@@ -296,10 +357,58 @@
         first, second = 2 * layer, 2 * layer + 1
         relay(first, 0, 1)
         drains.append(spreads[layer][1]())
-        normalize(layer)
+        if helped and layer == 0:
+            @pl.when(jnp.logical_not(is_end))
+            def _():
+                normalize(layer, layer, 0)
+        else:
+            normalize(layer, layer, 0)
         relay(first, 1, n)
-        wait_across(first)
-        project(layer)
+        relay(second, 0, 1)
+
+        def put(h, value):
+            pad[layer, PAD:PAD + rows, h * half:(h + 1) * half] = value
+
+        def put_out(h, value):
+            glu_out[:, h * half:(h + 1) * half] = value
+
+        if helped and layer == 0:
+            begin, finish = spread(xg, L, x_send, x_recv)
+
+            @pl.when(helper)
+            def _():
+                end_rows(end).wait_recv()
+                begin()
+                drain = finish()
+                normalize(0, L, 1)
+                for d in range(1, G):
+                    end_piece(d, lax.rem(g + d, G), end, end).wait_recv()
+                drain()
+
+            wait_across(first)
+
+            @pl.when(helper)
+            def _():
+                project(0, 1, put_out)
+                end_glu(end).start()
+
+            @pl.when(jnp.logical_not(is_end))
+            def _():
+                project(0, 0, put)
+
+            @pl.when(helper)
+            def _():
+                end_glu(end).wait_send()
+
+            @pl.when(is_end)
+            def _():
+                end_rows(inward).wait_send()
+                for d in range(1, G):
+                    end_piece(d, lax.rem(g + d, G), s, inward).wait_send()
+                end_glu(inward).wait_recv()
+        else:
+            wait_across(first)
+            project(layer, 0, put)
 
         def to_right():
             return pltpu.make_async_remote_copy(
@@ -329,7 +438,7 @@
         def _():
             pad[layer, PAD + rows:, :] = jnp.zeros((PAD, chans), bf16)
 
-        relay(second, 0, 1)
+        relay(second, 1, 2)
 
         @pl.when(s > 0)
         def _():
@@ -351,7 +460,6 @@
             sums.append(jnp.sum(total, axis=1, keepdims=True))
             squares.append(jnp.sum(total * total, axis=1, keepdims=True))
         totals = exchange(layer, [jnp.concatenate(sums, 0), jnp.concatenate(squares, 0)])
-        relay(second, 1, 2)
         total, square = totals()
         center = total / C
         spread_ = square / C - center * center
@@ -389,15 +497,17 @@
 
     def drain_step(j, carry):
         for p in range(L * pieces):
-            @pl.when((j <= s) & (s < n - 1))
+            came = (j == s) | takes(p)
+
+            @pl.when((j <= s) & to_right_ok(p) & came)
             def _():
                 right(p, j).wait_send()
 
-            @pl.when((j >= s) & (s > 0))
+            @pl.when((j >= s) & to_left_ok(p) & came)
             def _():
                 left(p, j).wait_send()
 
-            @pl.when(j != s)
+            @pl.when(by_grp(p, j))
             def _():
                 for d in range(1, G):
                     across(p, j, d, g).wait_send()
@@ -432,8 +542,9 @@
         scratch_shapes=[
             pltpu.VMEM((L, G, D, 2 * chans // G), bf16),
             pltpu.VMEM((L, G, C, width // G), bf16),
-            pltpu.VMEM((L, T, rows, width), bf16),
-            pltpu.VMEM((T, rows, width), bf16),
+            pltpu.VMEM((L + 1, T, rows, width), bf16),
+            pltpu.VMEM((2, T, rows, width), bf16),
+            pltpu.VMEM((rows, chans), bf16),
             pltpu.VMEM((rows, 2 * chans // G), f32),
             pltpu.VMEM((L, rows + 2 * PAD, chans), bf16),
             pltpu.VMEM((rows + 2 * PAD, chans), f32),
@@ -444,9 +555,10 @@
             dma((1 + L * G * 3,)),
             dma((P_, n)), dma((P_, n)), dma((P_, n)),
             dma((P_, n, peers)), dma((P_, n, peers)),
-            dma((L, T)), dma((L, T)), dma((L, T)), dma((L, T)),
+            dma((L + 1, T)), dma((L + 1, T)), dma((L, T)), dma((L, T)),
             dma((L + 1, T)), dma((L + 1, T)),
             dma((L, 2)), dma((L, 2)),
+            dma((G + 1,)), dma((G + 1,)),
         ],
         compiler_params=pltpu.CompilerParams(
             collective_id=0, has_side_effects=True, vmem_limit_bytes=56 * 2**20

time: 140 us -> 154 us (1.10)
  Pallas kernels: 136 us -> 150 us
    pallas_call x1, Pallas kernels: 136 us -> 150 us  [on_device(): pl.pallas_call(functools.partial(kernel, G, n, T, L), out_shape=jax.Shape...]
where the time goes in v2:
time: 154 us; the launch traced here: 153 us
  Pallas kernels  150 us (97%)
  local copies, waits for them, and re-layouts  3.91 us (3%)
    pallas_call x1, Pallas kernels, on_device(): pl.pallas_call(functools.partial(kernel, G, n, T, L), out_shape=jax.Shape...  150 us

profile of v2, /device:TPU:0, one launch (start us, length us, event | category | flops | bytes accessed | tf_op | source)
XLA Modules:
  0.0 153.5 jit_solution(7668636391721638763)
XLA Ops:
  0.0 0.0 copy-start
  0.0 1.4 reshape.6.gain
  1.4 0.0 copy-done
  1.4 0.6 copy.9.taps
  2.0 149.5 %shard_map.82 = bf16[256,1024]{1,0:T(8,128)(2,1)} custom-call(bf16[256,1024]{1,0:T(8,128)(2,1)} %tokens.1, f32[8,1024]{1,0:T(8,128)} %reshape.6.gain, bf16[2,1024,256]{2,1,0:T(8,128)(2,1)} %value_w.1, bf16[2,1024,256]{2,1,0:T(8,128)(2,1)} %gate_w.1, f32[2,31,256]{2,1,0:T(8,128)} %copy.9.taps, f32[2,256]{1,0:T(2,128)} %cgain.1, bf16[2,256,1024]{2,1,0:T(8,128)(2,1)} %out_w.1, ...), custom_call_target="tpu_custom_call" | custom-call | tf_op jit(solution)/shard_map/pallas_call | solution.py:537
  151.6 1.9 %copy.11 = bf16[256,1024]{1,0:T(8,128)(2,1)} copy(bf16[256,1024]{1,0:T(8,128)(2,1)} %shard_map.82) | data formatting | bytes 1048576
Async XLA Ops:
  0.0 1.4 copy-start

commit v3 on v2

--- a/solution.py
+++ b/solution.py
@@ -355,7 +355,10 @@
 
     for layer in range(L):
         first, second = 2 * layer, 2 * layer + 1
-        relay(first, 0, 1)
+        if layer == 0:
+            relay(first, 0, 1)
+        else:
+            relay(first, 1, 2)
         drains.append(spreads[layer][1]())
         if helped and layer == 0:
             @pl.when(jnp.logical_not(is_end))
@@ -363,7 +366,14 @@
                 normalize(layer, layer, 0)
         else:
             normalize(layer, layer, 0)
-        relay(first, 1, n)
+        relay(first, 1 if layer == 0 else 2, n)
+        begin, finish = spread(xg, L, x_send, x_recv)
+        if helped and layer == 0:
+            @pl.when(helper)
+            def _():
+                end_rows(end).wait_recv()
+                begin()
+
         relay(second, 0, 1)
 
         def put(h, value):
@@ -373,12 +383,8 @@
             glu_out[:, h * half:(h + 1) * half] = value
 
         if helped and layer == 0:
-            begin, finish = spread(xg, L, x_send, x_recv)
-
             @pl.when(helper)
             def _():
-                end_rows(end).wait_recv()
-                begin()
                 drain = finish()
                 normalize(0, L, 1)
                 for d in range(1, G):
@@ -460,6 +466,9 @@
             sums.append(jnp.sum(total, axis=1, keepdims=True))
             squares.append(jnp.sum(total * total, axis=1, keepdims=True))
         totals = exchange(layer, [jnp.concatenate(sums, 0), jnp.concatenate(squares, 0)])
+        relay(second, 2, n)
+        if layer + 1 < L:
+            relay(second + 1, 0, 1)
         total, square = totals()
         center = total / C
         spread_ = square / C - center * center
@@ -468,7 +477,6 @@
         act_begin, act_finish = spread(actg, layer, a_send, a_recv)
         act_begin()
         drains.append(act_finish())
-        relay(second, 2, n)
         wait_across(second)
         for h in range(G):
             part = None

time: 154 us -> 127 us (0.82)
  Pallas kernels: 150 us -> 122 us
    pallas_call x1, Pallas kernels: 150 us -> 122 us  [on_device(): pl.pallas_call(functools.partial(kernel, G, n, T, L), out_shape=jax.Shape...]
where the time goes in v3:
time: 127 us; the launch traced here: 126 us
  Pallas kernels  122 us (96%)
  local copies, waits for them, and re-layouts  3.91 us (3%)
    pallas_call x1, Pallas kernels, on_device(): pl.pallas_call(functools.partial(kernel, G, n, T, L), out_shape=jax.Shape...  122 us

profile of v3, /device:TPU:0, one launch (start us, length us, event | category | flops | bytes accessed | tf_op | source)
XLA Modules:
  0.0 126.3 jit_solution(18178985592606857339)
XLA Ops:
  0.0 0.0 copy-start
  0.0 1.4 %reshape.6.gain = f32[8,1024]{1,0:T(8,128)} reshape(f32[2,4096]{1,0:T(2,128)} %param.9) | data formatting | bytes 65536 | tf_op jit(solution)/shard_map/reshape | solution.py:574
  1.4 0.0 copy-done
  1.4 0.6 copy.9.taps
  2.0 122.3 %shard_map.82 = bf16[256,1024]{1,0:T(8,128)(2,1)} custom-call(bf16[256,1024]{1,0:T(8,128)(2,1)} %tokens.1, f32[8,1024]{1,0:T(8,128)} %reshape.6.gain, bf16[2,1024,256]{2,1,0:T(8,128)(2,1)} %value_w.1, bf16[2,1024,256]{2,1,0:T(8,128)(2,1)} %gate_w.1, f32[2,31,256]{2,1,0:T(8,128)} %copy.9.taps, f32[2,256]{1,0:T(2,128)} %cgain.1, bf16[2,256,1024]{2,1,0:T(8,128)(2,1)} %out_w.1, ...), custom_call_target="tpu_custom_call" | custom-call | tf_op jit(solution)/shard_map/pallas_call | solution.py:545
  124.4 1.9 %copy.11 = bf16[256,1024]{1,0:T(8,128)(2,1)} copy(bf16[256,1024]{1,0:T(8,128)(2,1)} %shard_map.82) | data formatting | bytes 1048576
Async XLA Ops:
  0.0 1.4 %copy-start = (f32[2,31,256]{2,0,1:T(2,128)S(1)}, f32[2,31,256]{2,0,1:T(2,128)}, u32[]{:S(2)}) copy-start(f32[2,31,256]{2,0,1:T(2,128)} %param.12) | copy-start | bytes 190468
